TPU v7x, 32 devices: a whole 2x2x4 slice. The times are simulated.
32 devices in a mesh: grp: 2 (over y), sp: 4 (over z), tp: 4 (over x, core).
Axes of the slice: x: 2, y: 2, z: 4, core: 2. Of those that a mesh axis runs over, the one named last changes fastest.
Arguments:
- resid_in: bfloat16 [2048, 2048], P(('grp', 'sp', 'tp')), parts along dimension 0, may hold values from -6 to 6
- query_narrow: bfloat16 [2048, 8, 128], P(('grp', 'sp'), 'tp'), parts along dimension 0, may hold values from -512 to 512
- key_narrow: bfloat16 [2048, 4, 128], P(('grp', 'sp'), 'tp'), parts along dimension 0, may hold values from -512 to 512
- value_narrow: bfloat16 [2048, 4, 128], P(('grp', 'sp'), 'tp'), parts along dimension 0, may hold values from -6 to 6
- query_wide: bfloat16 [2048, 8, 256], P(('grp', 'sp'), 'tp'), parts along dimension 0, may hold values from -512 to 512
- key_wide: bfloat16 [2048, 4, 256], P(('grp', 'sp'), 'tp'), parts along dimension 0, may hold values from -512 to 512
- value_wide: bfloat16 [2048, 4, 128], P(('grp', 'sp'), 'tp'), parts along dimension 0, may hold values from -6 to 6
- lambda_narrow: float32 [8], P('tp'), may hold values from 0.3 to 0.8
- lambda_wide: float32 [8], P('tp'), may hold values from 0.3 to 0.8
- head_gain: float32 [128], replicated, may hold values from 0.1 to 1.9
- out_narrow: bfloat16 [1024, 2048], P('tp'), may hold values from -0.125 to 0.125
- out_wide: bfloat16 [1024, 2048], P('tp'), may hold values from -0.125 to 0.125
- norm_gain: bfloat16 [2048], replicated, may hold values from 0.099609375 to 1.8984375
- up_weight: bfloat16 [2048, 8192], P('sp', 'tp'), may hold values from -0.125 to 0.125
- down_weight: bfloat16 [8192, 2048], P('tp', 'sp'), may hold values from -0.0625 to 0.0625
Outputs:
- mixed_out: bfloat16 [2048, 2048], P(('grp', 'sp', 'tp')), parts along dimension 0
There are 2 independent parts, one for each index of `grp`. A program takes and returns all parts, laid end to end along the dimension named above; an argument that names none is the same for every part. Nothing has to cross between parts.
All inputs are finite; a program needn't handle non-finite values.
Results may differ from a plain program's by a relative error of at most 0.018.
Values may be sent and summed in bfloat16 or wider, within the bound.
A program may use at most 128 MiB of HBM per device.

v0:
```python
import math
import jax
import jax.numpy as jnp
from jax import lax
from jax.sharding import PartitionSpec as P

NORM_EPS = 1e-06
OUT_SCALE = 0.8


def empty_state(query, key_head_stack, value_width):
    row_count, head_count = (query.shape[0], query.shape[1])
    group_size = head_count // key_head_stack
    row_top = jnp.full((key_head_stack, group_size, 2, row_count), -jnp.inf, jnp.float32)
    row_total = jnp.zeros((key_head_stack, group_size, 2, row_count), jnp.float32)
    weighted_values = jnp.zeros(
        (key_head_stack, group_size, 2, row_count, value_width), jnp.float32
    )
    return (row_top, row_total, weighted_values)


def absorb(states, query, key_rows, values):
    row_count, head_count = (query.shape[0], query.shape[1])
    key_head_stack = key_rows.shape[1]
    half_width = key_rows.shape[2] // 2
    group_size = head_count // key_head_stack
    value_width = values.shape[2]
    amount = key_rows.shape[0]
    block_rows = math.gcd(amount, 512)
    rotation_count = amount // block_rows
    grouped = query.reshape(row_count, key_head_stack, group_size, 2, half_width)
    key_block_list = key_rows.reshape(rotation_count, block_rows, key_head_stack, 2, half_width)
    value_blocks = values.reshape(rotation_count, block_rows, key_head_stack, value_width)

    def visit(running, kv_pair):
        row_top, row_total, weighted_values = running
        key_blk, value_blk = kv_pair
        scores = jnp.einsum(
            "tkgcd,skcd->kgcts", grouped, key_blk, preferred_element_type=jnp.float32
        ) * half_width ** (-0.5)
        new_top = jnp.maximum(row_top, jnp.max(scores, axis=-1))
        rescale = jnp.exp(row_top - new_top)
        powers = jnp.exp(scores - new_top[..., None])
        row_total = row_total * rescale + jnp.sum(powers, axis=-1)
        weighted_values = weighted_values * rescale[..., None] + jnp.einsum(
            "iodph,hie->iodpe",
            powers.astype(jnp.bfloat16),
            value_blk,
            preferred_element_type=jnp.float32,
        )
        return ((new_top, row_total, weighted_values), None)

    outcome, _ = lax.scan(visit, states, (key_block_list, value_blocks))
    return outcome


def finish(states, lambdas, gain_vec):
    row_top, row_total, weighted_values = states
    key_head_stack, group_size, row_count = (row_top.shape[0], row_top.shape[1], row_top.shape[3])
    value_width = weighted_values.shape[4]
    first_map = weighted_values[:, :, 0] / row_total[:, :, 0, :, None]
    second_map = weighted_values[:, :, 1] / row_total[:, :, 1, :, None]
    mixed = first_map - lambdas.reshape(key_head_stack, group_size)[:, :, None, None] * second_map
    normed = (
        mixed
        * lax.rsqrt(jnp.mean(mixed * mixed, axis=-1, keepdims=True) + NORM_EPS)
        * gain_vec
        * OUT_SCALE
    )
    normed = normed.astype(jnp.bfloat16).transpose(2, 0, 1, 3)
    return normed.reshape(row_count, key_head_stack * group_size * value_width)


def attend(
    query_narrow,
    key_narrow,
    value_narrow,
    query_wide,
    key_wide,
    value_wide,
    lambda_narrow,
    lambda_wide,
    head_gain,
):
    initial = (
        empty_state(query_narrow, key_narrow.shape[1], value_narrow.shape[2]),
        empty_state(query_wide, key_wide.shape[1], value_wide.shape[2]),
    )
    narrow_keys = lax.all_gather(key_narrow, "sp", axis=0, tiled=True)
    narrow_values = lax.all_gather(value_narrow, "sp", axis=0, tiled=True)
    wide_keys = lax.all_gather(key_wide, "sp", axis=0, tiled=True)
    wide_values = lax.all_gather(value_wide, "sp", axis=0, tiled=True)
    narrow_state = absorb(initial[0], query_narrow, narrow_keys, narrow_values)
    wide_state = absorb(initial[1], query_wide, wide_keys, wide_values)
    return (
        finish(narrow_state, lambda_narrow, head_gain),
        finish(wide_state, lambda_wide, head_gain),
    )


def shards(
    resid_in,
    query_narrow,
    key_narrow,
    value_narrow,
    query_wide,
    key_wide,
    value_wide,
    lambda_narrow,
    lambda_wide,
    head_gain,
    out_narrow,
    out_wide,
    norm_gain,
    up_weight,
    down_weight,
):
    att_narrow, att_wide = attend(
        query_narrow,
        key_narrow,
        value_narrow,
        query_wide,
        key_wide,
        value_wide,
        lambda_narrow,
        lambda_wide,
        head_gain,
    )
    projected = lax.psum_scatter(
        (
            jnp.dot(att_narrow, out_narrow, preferred_element_type=jnp.float32)
            + jnp.dot(att_wide, out_wide, preferred_element_type=jnp.float32)
        ).astype(jnp.bfloat16),
        "tp",
        scatter_dimension=0,
        tiled=True,
    ).astype(jnp.float32)
    middle = (resid_in.astype(jnp.float32) + projected).astype(jnp.bfloat16)
    middle_f32 = middle.astype(jnp.float32)
    normed = middle_f32 * lax.rsqrt(
        jnp.mean(middle_f32 * middle_f32, axis=-1, keepdims=True) + NORM_EPS
    )
    normed = (normed * norm_gain.astype(jnp.float32)).astype(jnp.bfloat16)
    whole_rows = lax.all_gather(normed, "tp", axis=0, tiled=True)
    up_collected = lax.all_gather(up_weight, "sp", axis=0, tiled=True)
    lifted = jnp.dot(whole_rows, up_collected, preferred_element_type=jnp.float32)
    activated = jnp.square(jax.nn.relu(lifted)).astype(jnp.bfloat16)
    partials = jnp.dot(
        activated,
        lax.all_gather(down_weight, "sp", axis=1, tiled=True),
        preferred_element_type=jnp.float32,
    )
    mixer_out = lax.psum_scatter(
        partials.astype(jnp.bfloat16), "tp", scatter_dimension=0, tiled=True
    ).astype(jnp.float32)
    return (middle_f32 + mixer_out).astype(jnp.bfloat16)


def solution(mesh):
    placed = (
        P(("grp", "sp", "tp"), None),
        P(("grp", "sp"), "tp", None),
        P(("grp", "sp"), "tp", None),
        P(("grp", "sp"), "tp", None),
        P(("grp", "sp"), "tp", None),
        P(("grp", "sp"), "tp", None),
        P(("grp", "sp"), "tp", None),
        P("tp"),
        P("tp"),
        P(),
        P("tp", None),
        P("tp", None),
        P(),
        P("sp", "tp"),
        P("tp", "sp"),
    )
    return jax.shard_map(
        shards, mesh=mesh, in_specs=placed, out_specs=P(("grp", "sp", "tp"), None), check_vma=False
    )
```

profile of v0, /device:TPU:0, one launch (start us, length us, event | category | flops | bytes accessed | tf_op | source)
XLA Modules:
  0.0 480.9 jit_solution(12649065433829812458)
XLA Ops:
  6.6 17.7 %all_gather.23 = bf16[1024,1,256]{2,0,1:T(8,128)(2,1)S(1)} all-gather(bf16[256,1,256]{2,0,1:T(8,128)(2,1)} %param.24), channel_id=1, replica_groups=mesh['grp'=2,'sp'=4,'tp'=4] {'sp'}, dimensions={0}, use_global_device_ids=true | all-gather | bytes 655360 | tf_op jit(solution)/shard_map/all_gather | solution.py:91
  24.4 1.1 copy.33
  25.5 0.2 copy.35
  25.7 15.3 %all_gather.24 = bf16[1024,1,128]{2,0,1:T(8,128)(2,1)} all-gather(bf16[256,1,128]{2,0,1:T(8,128)(2,1)S(1)} %copy-done.9), channel_id=1, replica_groups=mesh['grp'=2,'sp'=4,'tp'=4] {'sp'}, dimensions={0}, use_global_device_ids=true | all-gather | bytes 327680 | tf_op jit(solution)/shard_map/all_gather | solution.py:92
  41.1 8.2 %while.31 = (s32[]{:T(128)}, f32[1,2,2,256]{3,1,2,0:T(2,128)S(1)}, f32[1,2,2,256]{3,1,2,0:T(2,128)S(1)}, f32[1,2,2,256,128]{4,3,2,1,0:T(8,128)}, bf16[2,512,1,2,...) while((s32[]{:T(128)}, f32[1,2,2,256]{3,1,2,0:T(2,128)S(1)}, ...), condition=%wide.region_8.9_spmd.clone, body=%wide.region_5.0_spmd.clone.sunk | while | flops 271980544 | bytes 13832389 | solution.py:53
  41.1 0.2 constant_dynamic-slice_fusion.2
  41.3 0.6 copy-done.1
  41.9 0.4 bitcast_reduce_fusion.5
  42.4 0.4 fusion.71
  42.8 0.5 copy-done.7
  43.3 1.3 fusion.72
  44.7 0.2 constant_dynamic-slice_fusion.2
  44.9 0.6 copy-done.1
  45.5 0.4 bitcast_reduce_fusion.5
  46.0 0.4 fusion.71
  46.4 0.5 copy-done.7
  46.9 2.3 fusion.72
  49.3 0.6 slice_bitcast_fusion.5
  49.9 14.2 %all_gather.21 = bf16[1024,1,128]{2,0,1:T(8,128)(2,1)S(1)} all-gather(bf16[256,1,128]{2,0,1:T(8,128)(2,1)S(1)} %copy-done.10), channel_id=1, replica_groups=mesh['grp'=2,'sp'=4,'tp'=4] {'sp'}, dimensions={0}, use_global_device_ids=true | all-gather | bytes 327680 | tf_op jit(solution)/shard_map/all_gather | solution.py:89
  64.1 0.2 reshape.272
  64.3 0.4 copy.29
  64.7 15.6 %all_gather.22 = bf16[1024,1,128]{2,0,1:T(8,128)(2,1)} all-gather(bf16[256,1,128]{2,0,1:T(8,128)(2,1)} %param.22), channel_id=1, replica_groups=mesh['grp'=2,'sp'=4,'tp'=4] {'sp'}, dimensions={0}, use_global_device_ids=true | all-gather | bytes 327680 | tf_op jit(solution)/shard_map/all_gather | solution.py:90
  80.5 6.6 %while.30 = (s32[]{:T(128)}, f32[1,2,2,256]{3,1,2,0:T(2,128)S(1)}, f32[1,2,2,256]{3,1,2,0:T(2,128)S(1)}, f32[1,2,2,256,128]{4,3,2,1,0:T(8,128)}, bf16[2,512,1,2,...) while((s32[]{:T(128)}, f32[1,2,2,256]{3,1,2,0:T(2,128)S(1)}, ...), condition=%wide.region_3.4_spmd.clone, body=%wide.region_0.3_spmd.clone.sunk | while | flops 204871680 | bytes 8851597 | solution.py:53
  80.5 0.5 bitcast_reduce_fusion.4
  81.1 0.4 fusion.66
  81.5 0.5 copy-done.6
  82.0 1.3 fusion.67
  83.3 0.5 bitcast_reduce_fusion.4
  83.9 0.4 fusion.66
  84.3 0.5 copy-done.6
  84.8 2.3 fusion.67
  87.2 1.2 copy.36
  88.5 1.2 copy.31
  89.7 0.2 multiply_reduce_fusion
  90.1 0.5 fusion.45
  90.6 0.6 copy-done.5
  91.2 1.4 fusion.29
  92.7 25.0 %reduce-scatter.3.cloned.1.call-done = bf16[64,2048]{1,0:T(8,128)(2,1)} async-done(((bf16[256,2048]{1,0:T(8,128)(2,1)}), bf16[64,2048]{1,0:T(8,128)(2,1)}) %reduce-scatter.3.cloned.1.call-update) | async-done | bytes 262160 | tf_op jit(solution)/shard_map/reduce_scatter | solution.py:129
  117.7 1.1 fusion.30
  118.8 1.8 fusion.32
  120.7 0.7 all-gather.6.cloned.1.call-update
  121.4 0.5 all-gather.8.cloned.1.call-update
  122.0 15.5 %all-gather.4.cloned.1.call-done = bf16[256,2048]{1,0:T(8,128)(2,1)} async-done(((bf16[64,2048]{1,0:T(8,128)(2,1)}), bf16[256,2048]{1,0:T(8,128)(2,1)}) %all-gather.4.cloned.1.call-update) | async-done | bytes 1048592 | tf_op jit(solution)/shard_map/all_gather | solution.py:144
  137.4 151.2 %all-gather.6.cloned.1.call-done = bf16[2048,2048]{1,0:T(8,128)(2,1)} async-done(((bf16[512,2048]{1,0:T(8,128)(2,1)}), bf16[2048,2048]{1,0:T(8,128)(2,1)}) %all-gather.6.cloned.1.call-update) | async-done | bytes 8388624 | tf_op jit(solution)/shard_map/all_gather | solution.py:145
  288.7 149.3 %all-gather.8.cloned.1.call-done = bf16[2048,2048]{1,0:T(8,128)(2,1)} async-done(((bf16[2048,512]{1,0:T(8,128)(2,1)}), bf16[2048,2048]{1,0:T(8,128)(2,1)}) %all-gather.8.cloned.1.call-update) | async-done | bytes 8388624 | tf_op jit(solution)/shard_map/all_gather | solution.py:150
  437.9 11.5 %convolution_convert_fusion = bf16[256,2048]{1,0:T(8,128)(2,1)} fusion(bf16[2048,2048]{1,0:T(8,128)(2,1)} %all-gather.8.cloned.1.call-done, bf16[256,2048]{1,0:T(8,128)(2,1)} %all-gather.4.cloned.1.call-done, bf16[2048,2048]{1,0:T(8,128)(2,1)} %all-gather.6.cloned.1.call-done), kind=kOutput, calls=%fused_computation.52 | convolution fusion | flops 4297064448 | bytes 18874368 | tf_op jit(solution)/shard_map/dot_general | solution.py:148
  449.5 23.1 %reduce-scatter.5.cloned.1.call-done = bf16[64,2048]{1,0:T(8,128)(2,1)} async-done(((bf16[256,2048]{1,0:T(8,128)(2,1)}), bf16[64,2048]{1,0:T(8,128)(2,1)}) %reduce-scatter.5.cloned.1.call-update) | async-done | bytes 262160 | tf_op jit(solution)/shard_map/reduce_scatter | solution.py:153
  472.6 1.7 fusion.33
  (72 shorter events, 0.8 us)
Async XLA Ops:
  6.5 83.6 %copy-start = (bf16[256,2048]{1,0:T(8,128)(2,1)S(1)}, bf16[256,2048]{1,0:T(8,128)(2,1)}, u32[]{:S(2)}) copy-start(bf16[256,2048]{1,0:T(8,128)(2,1)} %param.29) | copy-start | bytes 3145732
  6.5 19.2 %copy-start.9 = (bf16[256,1,128]{2,0,1:T(8,128)(2,1)S(1)}, bf16[256,1,128]{2,0,1:T(8,128)(2,1)}, u32[]{:S(2)}) copy-start(bf16[256,1,128]{2,0,1:T(8,128)(2,1)} %param.25) | copy-start | bytes 196612
  6.5 111.1 %reduce-scatter.3.cloned.1.call-start = ((), (), s32[]{:S(2)}) async-start(), calls=%async_computation.2 | async-start | bytes 1310720 | tf_op jit(solution)/shard_map/reduce_scatter | solution.py:129
  41.1 8.8 %copy-start.10 = (bf16[256,1,128]{2,0,1:T(8,128)(2,1)S(1)}, bf16[256,1,128]{2,0,1:T(8,128)(2,1)}, u32[]{:S(2)}) copy-start(bf16[256,1,128]{2,0,1:T(8,128)(2,1)} %param.21) | copy-start | bytes 196612
  41.1 0.8 copy-start.1
  42.4 1.0 copy-start.7
  42.8 1.8 copy-start.2
  44.7 0.8 copy-start.1
  45.9 1.0 copy-start.7
  46.4 2.9 copy-start.2
  49.3 31.1 %copy-start.8 = (bf16[256,2,128]{2,1,0:T(2,128)(2,1)S(1)}, bf16[256,2,128]{2,1,0:T(2,128)(2,1)}, u32[]{:S(2)}) copy-start(bf16[256,2,128]{2,1,0:T(2,128)(2,1)} %param.20) | copy-start | bytes 393220
  81.0 1.0 copy-start.6
  83.8 1.0 copy-start.6
  87.2 2.6 copy-start.11
  87.2 2.6 copy-start.13
  87.2 2.6 copy-start.14
  87.2 2.8 copy-start.15
  89.9 1.2 copy-start.5
  91.2 1.5 copy-start.12
  91.2 26.5 %copy-start.3 = (bf16[64,2048]{1,0:T(8,128)(2,1)S(1)}, bf16[64,2048]{1,0:T(8,128)(2,1)}, u32[]{:S(2)}) copy-start(bf16[64,2048]{1,0:T(8,128)(2,1)} %param.19) | copy-start | bytes 786436
  92.6 44.8 %all-gather.4.cloned.1.call-start = ((), (), s32[]{:S(2)}) async-start(), calls=%async_computation.3 | async-start | bytes 1310720 | tf_op jit(solution)/shard_map/all_gather | solution.py:144
  120.6 168.1 %all-gather.6.cloned.1.call-start = ((), (), s32[]{:S(2)}) async-start(), calls=%async_computation.4 | async-start | bytes 10485760 | tf_op jit(solution)/shard_map/all_gather | solution.py:145
  121.3 316.6 %all-gather.8.cloned.1.call-start = ((), (), s32[]{:S(2)}) async-start(), calls=%async_computation.5 | async-start | bytes 10485760 | tf_op jit(solution)/shard_map/all_gather | solution.py:150
  121.9 350.7 %copy-start.4 = (bf16[64,2048]{1,0:T(8,128)(2,1)S(1)}, bf16[64,2048]{1,0:T(8,128)(2,1)}, u32[]{:S(2)}) copy-start(bf16[64,2048]{1,0:T(8,128)(2,1)} %reduce-scatter.3.cloned.1.call-done) | copy-start | bytes 786436
  121.9 350.7 %reduce-scatter.5.cloned.1.call-start = ((), (), s32[]{:S(2)}) async-start(), calls=%async_computation.6 | async-start | bytes 1310720 | tf_op jit(solution)/shard_map/reduce_scatter | solution.py:153
Sparse Core Ops, SparseCore 0:
  92.7 24.8 reduce-scatter.2
  120.7 16.6 all-gather.3
  139.0 149.6 all-gather.5
  290.1 147.7 all-gather.7
  449.6 22.9 reduce-scatter.4
where the time goes:
time: 481 us
  waiting for transfers between devices  365 us (76%)
  blocking collectives  62.9 us (13%)
  matrix products  22.6 us (5%)
  between operations  13.4 us (3%)
  local copies, waits for them, and re-layouts  9.51 us (2%)
  other arithmetic  6.74 us (1%)
    all_gather x1, waiting for transfers between devices, shards(): up_collected = lax.all_gather(up_weight, 'sp', axis=0, tiled=True)  151 us
    all_gather x1, waiting for transfers between devices, shards(): lax.all_gather(down_weight, 'sp', axis=1, tiled=True)  149 us
    reduce_scatter x1, waiting for transfers between devices, shards(): lax.psum_scatter((jnp.dot(att_narrow, out_narrow, preferred_element_type=...  25 us
    reduce_scatter x1, waiting for transfers between devices, shards(): lax.psum_scatter(partials.astype(jnp.bfloat16), 'tp', scatter_dimension=0...  23.1 us
    all_gather x1, blocking collectives, attend(): wide_keys = lax.all_gather(key_wide, 'sp', axis=0, tiled=True)  17.7 us
    all_gather x1, blocking collectives, attend(): narrow_values = lax.all_gather(value_narrow, 'sp', axis=0, tiled=True)  15.6 us
    all_gather x1, waiting for transfers between devices, shards(): whole_rows = lax.all_gather(normed, 'tp', axis=0, tiled=True)  15.5 us
    all_gather x1, blocking collectives, attend(): wide_values = lax.all_gather(value_wide, 'sp', axis=0, tiled=True)  15.3 us
  transfers between devices with their start and end apart: 5, of which 5 were waited for; matrix products, arithmetic and copies ran while one was open for 0% of the time, Pallas kernels for 0%

commit v1 on v0

--- a/solution.py
+++ b/solution.py
@@ -6,6 +6,17 @@
 
 NORM_EPS = 1e-06
 OUT_SCALE = 0.8
+
+
+def gather_by_hops(block, mesh_axis, along):
+    devices = lax.axis_size(mesh_axis)
+    hops = [(i, (i + 1) % devices) for i in range(devices)]
+    parts = [block]
+    for stride in range(1, devices):
+        parts = [lax.ppermute(parts[0], mesh_axis, hops), *parts]
+    whole = jnp.concatenate(parts, axis=along)
+    shift = (lax.axis_index(mesh_axis) + 1) * parts[-1].shape[along]
+    return jnp.roll(whole, shift, axis=along)
 
 
 def empty_state(query, key_head_stack, value_width):
@@ -142,7 +153,7 @@
     )
     normed = (normed * norm_gain.astype(jnp.float32)).astype(jnp.bfloat16)
     whole_rows = lax.all_gather(normed, "tp", axis=0, tiled=True)
-    up_collected = lax.all_gather(up_weight, "sp", axis=0, tiled=True)
+    up_collected = gather_by_hops(up_weight, "sp", 0)
     lifted = jnp.dot(whole_rows, up_collected, preferred_element_type=jnp.float32)
     activated = jnp.square(jax.nn.relu(lifted)).astype(jnp.bfloat16)
     partials = jnp.dot(

time: 481 us -> 458 us (0.952)
  waiting for transfers between devices: 365 us -> 249 us
  starting transfers between devices: 0.16 us -> 72.7 us
  local copies, waits for them, and re-layouts: 9.51 us -> 29.7 us
    ppermute x0 -> x3, waiting for transfers between devices: none -> 200 us  [gather_by_hops(): parts = [lax.ppermute(parts[0], mesh_axis, hops), *parts]]
    all_gather x1 -> x0, waiting for transfers between devices: 151 us -> none  [shards(): up_collected = lax.all_gather(up_weight, 'sp', axis=0, tiled=True)]
    all_gather x1, waiting for transfers between devices: 149 us -> 0.01 us  [shards(): lax.all_gather(down_weight, 'sp', axis=1, tiled=True)]
    ppermute x0 -> x3, starting transfers between devices: none -> 72.6 us  [gather_by_hops(): parts = [lax.ppermute(parts[0], mesh_axis, hops), *parts]]
    unnamed x29 -> x42, local copies, waits for them, and re-layouts: 2.43 us -> 21.2 us
    all_gather x1, waiting for transfers between devices: 15.5 us -> 0.01 us  [shards(): whole_rows = lax.all_gather(normed, 'tp', axis=0, tiled=True)]
  transfers between devices with their start and end apart: 5 -> 7, of which waited for: 5 -> 5; matrix products, arithmetic and copies ran while one was open for 0% -> 4% of each run, Pallas kernels for 0% -> 0%
where the time goes in v1:
time: 458 us; the launch traced here: 457 us
  waiting for transfers between devices  249 us (54%)
  starting transfers between devices  72.7 us (16%)
  blocking collectives  62.9 us (14%)
  local copies, waits for them, and re-layouts  29.7 us (6%)
  matrix products  22.8 us (5%)
  between operations  13.4 us (3%)
  other arithmetic  6.74 us (1%)
    ppermute x3, waiting for transfers between devices, gather_by_hops(): parts = [lax.ppermute(parts[0], mesh_axis, hops), *parts]  200 us
    ppermute x3, starting transfers between devices, gather_by_hops(): parts = [lax.ppermute(parts[0], mesh_axis, hops), *parts]  72.6 us
    reduce_scatter x1, waiting for transfers between devices, shards(): lax.psum_scatter((jnp.dot(att_narrow, out_narrow, preferred_element_type=...  24.9 us
    reduce_scatter x1, waiting for transfers between devices, shards(): lax.psum_scatter(partials.astype(jnp.bfloat16), 'tp', scatter_dimension=0...  22.8 us
    unnamed x42, local copies, waits for them, and re-layouts  21.2 us
    all_gather x1, blocking collectives, attend(): wide_keys = lax.all_gather(key_wide, 'sp', axis=0, tiled=True)  17.7 us
    all_gather x1, blocking collectives, attend(): narrow_values = lax.all_gather(value_narrow, 'sp', axis=0, tiled=True)  15.7 us
    all_gather x1, blocking collectives, attend(): wide_values = lax.all_gather(value_wide, 'sp', axis=0, tiled=True)  15.3 us
  transfers between devices with their start and end apart: 7, of which 5 were waited for; matrix products, arithmetic and copies ran while one was open for 4% of the time, Pallas kernels for 0%

profile of v1, /device:TPU:0, one launch (start us, length us, event | category | flops | bytes accessed | tf_op | source)
XLA Modules:
  0.0 457.2 jit_solution(2606042599777396389)
XLA Ops:
  6.6 17.7 %all_gather.20 = bf16[1024,1,256]{2,0,1:T(8,128)(2,1)S(1)} all-gather(bf16[256,1,256]{2,0,1:T(8,128)(2,1)} %param.24), channel_id=1, replica_groups=mesh['grp'=2,'sp'=4,'tp'=4] {'sp'}, dimensions={0}, use_global_device_ids=true | all-gather | bytes 655360 | tf_op jit(solution)/shard_map/all_gather | solution.py:102
  24.4 1.1 copy.33
  25.7 15.3 %all_gather.21 = bf16[1024,1,128]{2,0,1:T(8,128)(2,1)} all-gather(bf16[256,1,128]{2,0,1:T(8,128)(2,1)S(1)} %copy-done.12), channel_id=1, replica_groups=mesh['grp'=2,'sp'=4,'tp'=4] {'sp'}, dimensions={0}, use_global_device_ids=true | all-gather | bytes 327680 | tf_op jit(solution)/shard_map/all_gather | solution.py:103
  41.1 8.2 %while.31 = (s32[]{:T(128)}, f32[1,2,2,256]{3,1,2,0:T(2,128)S(1)}, f32[1,2,2,256]{3,1,2,0:T(2,128)S(1)}, f32[1,2,2,256,128]{4,3,2,1,0:T(8,128)}, bf16[2,512,1,2,...) while((s32[]{:T(128)}, f32[1,2,2,256]{3,1,2,0:T(2,128)S(1)}, ...), condition=%wide.region_8.9_spmd.clone, body=%wide.region_5.0_spmd.clone.sunk | while | flops 271980544 | bytes 13832389 | solution.py:64
  41.3 0.6 copy-done.4
  41.9 0.4 bitcast_reduce_fusion.5
  42.8 0.5 copy-done.9
  43.3 1.3 fusion.84
  44.9 0.6 copy-done.4
  46.4 0.5 copy-done.9
  46.9 2.3 fusion.84
  49.3 0.6 slice_bitcast_fusion.5
  49.9 14.2 %all_gather.18 = bf16[1024,1,128]{2,0,1:T(8,128)(2,1)S(1)} all-gather(bf16[256,1,128]{2,0,1:T(8,128)(2,1)S(1)} %copy-done.13), channel_id=1, replica_groups=mesh['grp'=2,'sp'=4,'tp'=4] {'sp'}, dimensions={0}, use_global_device_ids=true | all-gather | bytes 327680 | tf_op jit(solution)/shard_map/all_gather | solution.py:100
  64.7 15.7 %all_gather.19 = bf16[1024,1,128]{2,0,1:T(8,128)(2,1)} all-gather(bf16[256,1,128]{2,0,1:T(8,128)(2,1)} %param.22), channel_id=1, replica_groups=mesh['grp'=2,'sp'=4,'tp'=4] {'sp'}, dimensions={0}, use_global_device_ids=true | all-gather | bytes 327680 | tf_op jit(solution)/shard_map/all_gather | solution.py:101
  80.5 6.7 %while.30 = (s32[]{:T(128)}, f32[1,2,2,256]{3,1,2,0:T(2,128)S(1)}, f32[1,2,2,256]{3,1,2,0:T(2,128)S(1)}, f32[1,2,2,256,128]{4,3,2,1,0:T(8,128)}, bf16[2,512,1,2,...) while((s32[]{:T(128)}, f32[1,2,2,256]{3,1,2,0:T(2,128)S(1)}, ...), condition=%wide.region_3.4_spmd.clone, body=%wide.region_0.3_spmd.clone.sunk | while | flops 204871680 | bytes 8851597 | solution.py:64
  80.5 0.5 bitcast_reduce_fusion.4
  81.4 0.5 copy-done.10
  82.0 1.3 fusion.79
  83.3 0.5 bitcast_reduce_fusion.4
  84.3 0.5 copy-done.10
  84.8 2.3 fusion.79
  87.2 1.2 copy.36
  88.4 1.2 copy.31
  90.1 0.5 fusion.58
  90.5 0.6 copy-done.8
  91.1 1.5 fusion.35
  92.7 24.9 %reduce-scatter.3.cloned.1.call-done = bf16[64,2048]{1,0:T(8,128)(2,1)} async-done(((bf16[256,2048]{1,0:T(8,128)(2,1)}), bf16[64,2048]{1,0:T(8,128)(2,1)}) %reduce-scatter.3.cloned.1.call-update) | async-done | bytes 262160 | tf_op jit(solution)/shard_map/reduce_scatter | solution.py:140
  117.6 1.1 fusion.41
  118.8 1.8 fusion.43
  120.6 0.7 all-gather.5.cloned.1.call-update
  121.4 1.6 collective-permute-start
  122.9 66.2 %collective-permute-done = bf16[512,2048]{1,0:T(8,128)(2,1)S(1)} collective-permute-done((bf16[512,2048]{1,0:T(8,128)(2,1)S(1)}, bf16[512,2048]{1,0:T(8,128)(2,1)S(1)}, u32[]{:S(2)}, u32[]{:S(2)}) %collective-permute-start) | collective-permute-done | bytes 2097184 | tf_op jit(solution)/shard_map/ppermute | solution.py:16
  189.1 1.4 copy-done.2
  190.5 21.8 %collective-permute-start.1 = (bf16[512,2048]{1,0:T(8,128)(2,1)S(1)}, bf16[512,2048]{1,0:T(8,128)(2,1)}, u32[]{:S(2)}, u32[]{:S(2)}) collective-permute-start(bf16[512,2048]{1,0:T(8,128)(2,1)S(1)} %collective-permute-done), channel_id=1, source_target_pairs={{0,4},{4,8},{8,12},{12,0},{1,5},{5,9},{9,13},{13,1},{2,6},{6,10},{... | collective-permute-start | bytes 6291464 | tf_op jit(solution)/shard_map/ppermute | solution.py:16
  212.3 88.8 %collective-permute-done.1 = bf16[512,2048]{1,0:T(8,128)(2,1)} collective-permute-done((bf16[512,2048]{1,0:T(8,128)(2,1)S(1)}, bf16[512,2048]{1,0:T(8,128)(2,1)}, u32[]{:S(2)}, u32[]{:S(2)}) %collective-permute-start.1) | collective-permute-done | bytes 2097184 | tf_op jit(solution)/shard_map/ppermute | solution.py:16
  301.1 49.2 %collective-permute-start.2 = (bf16[512,2048]{1,0:T(8,128)(2,1)}, bf16[512,2048]{1,0:T(8,128)(2,1)}, u32[]{:S(2)}, u32[]{:S(2)}) collective-permute-start(bf16[512,2048]{1,0:T(8,128)(2,1)} %collective-permute-done.1), channel_id=1, source_target_pairs={{0,4},{4,8},{8,12},{12,0},{1,5},{5,9},{9,13},{13,1},{2,6},{6,10},{... | collective-permute-start | bytes 6291464 | tf_op jit(solution)/shard_map/ppermute | solution.py:16
  350.3 45.3 %collective-permute-done.2 = bf16[512,2048]{1,0:T(8,128)(2,1)} collective-permute-done((bf16[512,2048]{1,0:T(8,128)(2,1)}, bf16[512,2048]{1,0:T(8,128)(2,1)}, u32[]{:S(2)}, u32[]{:S(2)}) %collective-permute-start.2) | collective-permute-done | bytes 2097184 | tf_op jit(solution)/shard_map/ppermute | solution.py:16
  395.6 3.2 constant_dynamic-update-slice_fusion.7
  398.8 3.3 constant_dynamic-update-slice_fusion.6
  402.1 1.5 constant_dynamic-update-slice_fusion.5
  403.6 1.5 constant_dynamic-update-slice_fusion.4
  405.1 3.2 constant_dynamic-update-slice_fusion.3
  408.3 3.2 constant_dynamic-update-slice_fusion.2
  411.5 1.5 constant_dynamic-update-slice_fusion.1
  413.0 1.4 constant_dynamic-update-slice_fusion
  414.4 11.7 %convolution_convert_fusion = bf16[256,2048]{1,0:T(8,128)(2,1)} fusion(bf16[2048,2048]{1,0:T(8,128)(2,1)} %all-gather.5.cloned.1.call-done, bf16[256,2048]{1,0:T(8,128)(2,1)} %all-gather.3.cloned.1.call-done, bf16[4096,2048]{1,0:T(8,128)(2,1)} %constant_dynamic-update-slice_fusion, s32[]{:T(128)S(6)} %select_n.14), kind=kOutput, calls=%fused_computation.54 | convolution fusion | flops 4297064448 | bytes 18874372 | tf_op jit(solution)/shard_map/dot_general | solution.py:159
  426.1 22.8 %reduce-scatter.5.cloned.1.call-done = bf16[64,2048]{1,0:T(8,128)(2,1)} async-done(((bf16[256,2048]{1,0:T(8,128)(2,1)}), bf16[64,2048]{1,0:T(8,128)(2,1)}) %reduce-scatter.5.cloned.1.call-update) | async-done | bytes 262160 | tf_op jit(solution)/shard_map/reduce_scatter | solution.py:164
  448.9 1.7 fusion.44
  (89 shorter events, 4.2 us)
Async XLA Ops:
  6.5 83.5 %copy-start = (bf16[256,2048]{1,0:T(8,128)(2,1)S(1)}, bf16[256,2048]{1,0:T(8,128)(2,1)}, u32[]{:S(2)}) copy-start(bf16[256,2048]{1,0:T(8,128)(2,1)} %param.29) | copy-start | bytes 3145732
  6.5 19.2 %copy-start.12 = (bf16[256,1,128]{2,0,1:T(8,128)(2,1)S(1)}, bf16[256,1,128]{2,0,1:T(8,128)(2,1)}, u32[]{:S(2)}) copy-start(bf16[256,1,128]{2,0,1:T(8,128)(2,1)} %param.25) | copy-start | bytes 196612
  6.5 111.1 %reduce-scatter.3.cloned.1.call-start = ((), (), s32[]{:S(2)}) async-start(), calls=%async_computation.2 | async-start | bytes 1310720 | tf_op jit(solution)/shard_map/reduce_scatter | solution.py:140
  41.1 8.8 %copy-start.13 = (bf16[256,1,128]{2,0,1:T(8,128)(2,1)S(1)}, bf16[256,1,128]{2,0,1:T(8,128)(2,1)}, u32[]{:S(2)}) copy-start(bf16[256,1,128]{2,0,1:T(8,128)(2,1)} %param.21) | copy-start | bytes 196612
  41.1 0.8 copy-start.4
  42.4 1.0 copy-start.9
  42.8 1.8 copy-start.5
  44.7 0.8 copy-start.4
  45.9 1.0 copy-start.9
  46.4 2.9 copy-start.5
  49.3 31.1 %copy-start.11 = (bf16[256,2,128]{2,1,0:T(2,128)(2,1)S(1)}, bf16[256,2,128]{2,1,0:T(2,128)(2,1)}, u32[]{:S(2)}) copy-start(bf16[256,2,128]{2,1,0:T(2,128)(2,1)} %param.20) | copy-start | bytes 393220
  81.0 1.0 copy-start.10
  83.8 1.0 copy-start.10
  87.1 2.6 copy-start.14
  87.1 2.6 copy-start.16
  87.2 2.6 copy-start.17
  87.2 2.8 copy-start.18
  89.9 1.2 copy-start.8
  91.1 1.5 copy-start.15
  91.1 26.5 %copy-start.6 = (bf16[64,2048]{1,0:T(8,128)(2,1)S(1)}, bf16[64,2048]{1,0:T(8,128)(2,1)}, u32[]{:S(2)}) copy-start(bf16[64,2048]{1,0:T(8,128)(2,1)} %param.19) | copy-start | bytes 786436
  92.6 28.7 %copy-start.1 = (bf16[512,2048]{1,0:T(8,128)(2,1)S(1)}, bf16[512,2048]{1,0:T(8,128)(2,1)}, u32[]{:S(2)}) copy-start(bf16[512,2048]{1,0:T(8,128)(2,1)} %param.32) | copy-start | bytes 6291460
  92.6 321.8 %all-gather.3.cloned.1.call-start = ((), (), s32[]{:S(2)}) async-start(), calls=%async_computation.3 | async-start | bytes 1310720 | tf_op jit(solution)/shard_map/all_gather | solution.py:155
  120.6 293.8 %all-gather.5.cloned.1.call-start = ((), (), s32[]{:S(2)}) async-start(), calls=%async_computation.4 | async-start | bytes 10485760 | tf_op jit(solution)/shard_map/all_gather | solution.py:161
  121.3 327.6 %reduce-scatter.5.cloned.1.call-start = ((), (), s32[]{:S(2)}) async-start(), calls=%async_computation.5 | async-start | bytes 1310720 | tf_op jit(solution)/shard_map/reduce_scatter | solution.py:164
  121.4 67.8 %collective-permute-start = (bf16[512,2048]{1,0:T(8,128)(2,1)S(1)}, bf16[512,2048]{1,0:T(8,128)(2,1)S(1)}, u32[]{:S(2)}, u32[]{:S(2)}) collective-permute-start(bf16[512,2048]{1,0:T(8,128)(2,1)S(1)} %copy-done.1), channel_id=1, source_target_pairs={{0,4},{4,8},{8,12},{12,0},{1,5},{5,9},{9,13},{13,1},{2,6},{6,10},{... | collective-permute-start | bytes 6291464 | tf_op jit(solution)/shard_map/ppermute | solution.py:16
  189.1 1.4 copy-start.2
  190.5 110.6 %collective-permute-start.1 = (bf16[512,2048]{1,0:T(8,128)(2,1)S(1)}, bf16[512,2048]{1,0:T(8,128)(2,1)}, u32[]{:S(2)}, u32[]{:S(2)}) collective-permute-start(bf16[512,2048]{1,0:T(8,128)(2,1)S(1)} %collective-permute-done), channel_id=1, source_target_pairs={{0,4},{4,8},{8,12},{12,0},{1,5},{5,9},{9,13},{13,1},{2,6},{6,10},{... | collective-permute-start | bytes 6291464 | tf_op jit(solution)/shard_map/ppermute | solution.py:16
  301.1 94.5 %collective-permute-start.2 = (bf16[512,2048]{1,0:T(8,128)(2,1)}, bf16[512,2048]{1,0:T(8,128)(2,1)}, u32[]{:S(2)}, u32[]{:S(2)}) collective-permute-start(bf16[512,2048]{1,0:T(8,128)(2,1)} %collective-permute-done.1), channel_id=1, source_target_pairs={{0,4},{4,8},{8,12},{12,0},{1,5},{5,9},{9,13},{13,1},{2,6},{6,10},{... | collective-permute-start | bytes 6291464 | tf_op jit(solution)/shard_map/ppermute | solution.py:16
  398.8 3.3 copy-start.3
  414.4 34.5 %copy-start.7 = (bf16[64,2048]{1,0:T(8,128)(2,1)S(1)}, bf16[64,2048]{1,0:T(8,128)(2,1)}, u32[]{:S(2)}) copy-start(bf16[64,2048]{1,0:T(8,128)(2,1)} %reduce-scatter.3.cloned.1.call-done) | copy-start | bytes 786436
Sparse Core Ops, SparseCore 0:
  92.7 24.8 reduce-scatter.2
  120.7 16.7 all-gather.2
  139.0 214.4 all-gather.4
  426.2 22.6 reduce-scatter.4
